TPU v7x, 32 devices: a whole 2x2x4 slice. The times are simulated.
32 devices in a mesh: sp: 4 (over z), tp: 4 (over y, x), dp: 2 (over core).
Axes of the slice: x: 2, y: 2, z: 4, core: 2. Of those that a mesh axis runs over, the one named last changes fastest.
Arguments:
- latent_in: bfloat16 [3072, 2048], P(('dp', 'sp', 'tp')), parts along dimension 0, may hold values from -6 to 6
- condition: bfloat16 [4096], P(('dp', 'sp')), parts along dimension 0, may hold values from -8 to 8
- context_latent: bfloat16 [1024, 256], P(('dp', 'sp')), parts along dimension 0, may hold values from -6 to 6
- context_rope: bfloat16 [1024, 64], P(('dp', 'sp')), parts along dimension 0, may hold values from -6 to 6
- shift_weight: bfloat16 [2048, 2048], P('sp', 'tp'), may hold values from -0.125 to 0.125
- scale_weight: bfloat16 [2048, 2048], P('sp', 'tp'), may hold values from -0.125 to 0.125
- gate_weight: bfloat16 [2048, 2048], P('sp', 'tp'), may hold values from -0.125 to 0.125
- norm_gain: float32 [2048], replicated, may hold values from 0.1 to 1.9
- down_query: bfloat16 [2048, 512], replicated, may hold values from -0.125 to 0.125
- down_latent: bfloat16 [2048, 256], replicated, may hold values from -0.125 to 0.125
- down_rope: bfloat16 [2048, 64], replicated, may hold values from -0.125 to 0.125
- query_gain: float32 [512], replicated, may hold values from 0.5 to 60
- latent_gain: float32 [256], replicated, may hold values from 0.1 to 1.9
- up_query: bfloat16 [512, 1536], P(None, 'tp'), may hold values from -0.25 to 0.25
- up_key: bfloat16 [256, 1024], P(None, 'tp'), may hold values from -0.375 to 0.375
- up_value: bfloat16 [256, 1024], P(None, 'tp'), may hold values from -0.375 to 0.375
- context_bias: float32 [8], P('tp'), may hold values from 1 to 2.5
- out_weight: bfloat16 [1024, 2048], replicated, may hold values from -3 to 3
Outputs:
- mixed_out: bfloat16 [3072, 2048], P(('dp', 'sp', 'tp')), parts along dimension 0
There are 2 independent parts, one for each index of `dp`. A program takes and returns all parts, laid end to end along the dimension named above; an argument that names none is the same for every part. Nothing has to cross between parts.
All inputs are finite; a program needn't handle non-finite values.
Results may differ from a plain program's by a relative error of at most 0.039.
The roundings to bfloat16 on the way count: a program that leaves them out, or rounds other values in their place, can miss the bound.
Values may be sent and summed in bfloat16 or wider, within the bound.
A program may use at most 128 MiB of HBM per device.

v0:
```python
import jax
import jax.numpy as jnp
from jax import lax
from jax.sharding import PartitionSpec as P

QK_NOPE = 128
QK_ROPE = 64
V_HEAD = 128
GRID_W = 64
epsilon = 1e-06
rope_base = 10000.0
block_limit = 2048


def rms_scaled(values, gain_vec):
    mean_sq = jnp.mean(values * values, axis=-1, keepdims=True)
    return values * lax.rsqrt(mean_sq + epsilon) * gain_vec


def rope_tables(positions, rope_width):
    freq_count = rope_width // 4
    inverse = rope_base ** (-jnp.arange(freq_count, dtype=jnp.float32) / freq_count)
    grid_row = (positions // GRID_W).astype(jnp.float32)
    grid_col = (positions % GRID_W).astype(jnp.float32)
    row_angle = grid_row[:, None] * inverse
    col_angle = grid_col[:, None] * inverse
    angles = jnp.concatenate([row_angle, row_angle, col_angle, col_angle], axis=-1)
    return (jnp.cos(angles), jnp.sin(angles))


def rope_turn(values, cosine_table, sine_table):
    part_one, part_two, part_three, part_four = jnp.split(values, 4, axis=-1)
    turned = jnp.concatenate([-part_two, part_one, -part_four, part_three], axis=-1)
    return values * cosine_table + turned * sine_table


def attend(attn_state, query_nope, query_rope, keys_nope, values_in, keys_rope, bias_col):
    score_scale = (query_nope.shape[-1] + query_rope.shape[-1]) ** (-0.5)
    scores = jnp.einsum("thd,khd->htk", query_nope, keys_nope, preferred_element_type=jnp.float32)
    scores = scores + jnp.einsum(
        "thr,kr->htk", query_rope, keys_rope, preferred_element_type=jnp.float32
    )
    scores = scores * score_scale + bias_col
    run_max, run_total, run_acc = attn_state
    new_max = jnp.maximum(run_max, jnp.max(scores, axis=-1))
    shrink = jnp.exp(run_max - new_max)
    weights = jnp.exp(scores - new_max[:, :, None])
    new_total = run_total * shrink + jnp.sum(weights, axis=-1)
    new_acc = run_acc * shrink[:, :, None] + jnp.einsum(
        "htk,khd->htd", weights.astype(jnp.bfloat16), values_in, preferred_element_type=jnp.float32
    )
    return (new_max, new_total, new_acc)


def over_blocks(attn_state, arrays, handle):
    row_count = arrays[0].shape[0]
    block_rows = 1
    for candidate in range(min(row_count, block_limit), 0, -1):
        if row_count % candidate == 0:
            block_rows = candidate
            break
    block_count = row_count // block_rows
    if block_count == 1:
        return handle(attn_state, arrays)
    stacked = tuple(
        (array_in.reshape((block_count, block_rows) + array_in.shape[1:]) for array_in in arrays)
    )

    def one_turn(inner_state, pieces):
        return (handle(inner_state, pieces), None)

    return lax.scan(one_turn, attn_state, stacked)[0]


def on_device(
    latent_in,
    condition,
    context_latent,
    context_rope,
    shift_weight,
    scale_weight,
    gate_weight,
    norm_gain,
    down_query,
    down_latent,
    down_rope,
    query_gain,
    latent_gain,
    up_query,
    up_key,
    up_value,
    context_bias,
    out_weight,
):
    activated = jax.nn.silu(condition.astype(jnp.float32)).astype(jnp.bfloat16)
    partials = jnp.stack(
        [
            jnp.dot(activated, weight_in, preferred_element_type=jnp.float32)
            for weight_in in (shift_weight, scale_weight, gate_weight)
        ]
    )
    summed = lax.psum(partials, "sp")
    modulation = lax.all_gather(summed, "tp", axis=1, tiled=True)
    shift_vec = modulation[0]
    scale_vec = modulation[1]
    gate_vec = modulation[2]
    residual_in = latent_in.astype(jnp.float32)
    normed = (rms_scaled(residual_in, norm_gain) * (1.0 + scale_vec) + shift_vec).astype(
        jnp.bfloat16
    )
    query_low = rms_scaled(
        jnp.dot(normed, down_query, preferred_element_type=jnp.float32), query_gain
    ).astype(jnp.bfloat16)
    latent_low = rms_scaled(
        jnp.dot(normed, down_latent, preferred_element_type=jnp.float32), latent_gain
    ).astype(jnp.bfloat16)
    local_rows = latent_in.shape[0]
    first_row = (lax.axis_index("sp") * lax.axis_size("tp") + lax.axis_index("tp")) * local_rows
    own_positions = first_row + jnp.arange(local_rows, dtype=jnp.int32)
    own_cosine, own_sine = rope_tables(own_positions, QK_ROPE)
    rope_keys = rope_turn(
        jnp.dot(normed, down_rope, preferred_element_type=jnp.float32), own_cosine, own_sine
    ).astype(jnp.bfloat16)
    query_group, latent_group, rope_group = (
        lax.all_gather(query_low, "tp", axis=0, tiled=True),
        lax.all_gather(latent_low, "tp", axis=0, tiled=True),
        lax.all_gather(rope_keys, "tp", axis=0, tiled=True),
    )
    group_rows = query_group.shape[0]
    group_positions = lax.axis_index("sp") * group_rows + jnp.arange(group_rows, dtype=jnp.int32)
    group_cosine, group_sine = rope_tables(group_positions, QK_ROPE)
    head_count = up_key.shape[1] // QK_NOPE
    queries = jnp.dot(query_group, up_query, preferred_element_type=jnp.float32).reshape(
        group_rows, head_count, QK_NOPE + QK_ROPE
    )
    query_nope = queries[:, :, :QK_NOPE].astype(jnp.bfloat16)
    query_rope = rope_turn(
        queries[:, :, QK_NOPE:], group_cosine[:, None, :], group_sine[:, None, :]
    ).astype(jnp.bfloat16)
    context_all, context_keys_rope = (
        lax.all_gather(context_latent, "sp", axis=0, tiled=True),
        lax.all_gather(context_rope, "sp", axis=0, tiled=True),
    )
    context_count = context_all.shape[0]
    context_nope = (
        jnp.dot(context_all, up_key, preferred_element_type=jnp.float32)
        .astype(jnp.bfloat16)
        .reshape(context_count, head_count, QK_NOPE)
    )
    context_values = (
        jnp.dot(context_all, up_value, preferred_element_type=jnp.float32)
        .astype(jnp.bfloat16)
        .reshape(context_count, head_count, V_HEAD)
    )
    start_state = (
        jnp.full((head_count, group_rows), -jnp.inf, jnp.float32),
        jnp.zeros((head_count, group_rows), jnp.float32),
        jnp.zeros((head_count, group_rows, V_HEAD), jnp.float32),
    )
    bias_col = context_bias[:, None, None]

    def context_step(inner_state, pieces):
        return attend(
            inner_state, query_nope, query_rope, pieces[0], pieces[1], pieces[2], bias_col
        )

    attn_state = over_blocks(
        start_state, (context_nope, context_values, context_keys_rope), context_step
    )
    own_nope = jnp.dot(latent_group, up_key, preferred_element_type=jnp.float32).astype(
        jnp.bfloat16
    )
    own_values = jnp.dot(latent_group, up_value, preferred_element_type=jnp.float32).astype(
        jnp.bfloat16
    )

    def expanded_step(inner_state, pieces):
        piece_rows = pieces[0].shape[0]
        return attend(
            inner_state,
            query_nope,
            query_rope,
            pieces[0].reshape(piece_rows, head_count, QK_NOPE),
            pieces[1].reshape(piece_rows, head_count, V_HEAD),
            pieces[2],
            0.0,
        )

    attn_state = over_blocks(
        attn_state,
        (
            lax.all_gather(own_nope, "sp", axis=0, tiled=True),
            lax.all_gather(own_values, "sp", axis=0, tiled=True),
            lax.all_gather(rope_group, "sp", axis=0, tiled=True),
        ),
        expanded_step,
    )
    attended = (attn_state[2] / attn_state[1][:, :, None]).astype(jnp.bfloat16)
    attended = attended.transpose(1, 0, 2).reshape(group_rows, head_count * V_HEAD)
    token_major = lax.all_to_all(attended, "tp", split_axis=0, concat_axis=1, tiled=True)
    mixed = jnp.dot(token_major, out_weight, preferred_element_type=jnp.float32)
    return (residual_in + gate_vec * mixed).astype(jnp.bfloat16)


def solution(mesh):
    in_specs = (
        P(("dp", "sp", "tp"), None),
        P(("dp", "sp")),
        P(("dp", "sp"), None),
        P(("dp", "sp"), None),
        P("sp", "tp"),
        P("sp", "tp"),
        P("sp", "tp"),
        P(),
        P(),
        P(),
        P(),
        P(),
        P(),
        P(None, "tp"),
        P(None, "tp"),
        P(None, "tp"),
        P("tp"),
        P(),
    )
    out_specs = P(("dp", "sp", "tp"), None)
    return jax.shard_map(
        on_device, mesh=mesh, in_specs=in_specs, out_specs=out_specs, check_vma=False
    )
```

profile of v0, /device:TPU:0, one launch (start us, length us, event | category | flops | bytes accessed | tf_op | source)
XLA Modules:
  0.0 158.6 jit_solution(2897633564219635338)
XLA Ops:
  0.0 0.6 multiply_power_fusion
  0.6 0.7 fusion.54
  1.3 1.2 fusion.72
  2.6 1.2 fusion.73
  3.8 1.3 fusion.74
  5.1 13.8 %psum.7 = f32[3,512]{1,0:T(4,128)S(1)} all-reduce(f32[3,512]{1,0:T(4,128)S(1)} %pad_maximum_fusion.2), channel_id=1, replica_groups=mesh['sp'=4,'tp'=4,'dp'=2] {'sp'}, use_global_device_ids=true, to_apply=%region_0.1 | all-reduce | flops 1536 | bytes 12288 | tf_op jit(solution)/shard_map/psum | solution.py:102
  18.9 8.2 %all_gather.27 = f32[3,2048]{1,0:T(4,128)S(1)} all-gather(f32[3,512]{1,0:T(4,128)S(1)} %psum.7), channel_id=1, replica_groups=mesh['sp'=4,'tp'=4,'dp'=2] {'tp'}, dimensions={1}, use_global_device_ids=true | all-gather | bytes 30720 | tf_op jit(solution)/shard_map/all_gather | solution.py:103
  27.1 1.2 fusion.26
  28.4 1.9 %multiply_reduce_fusion.1 = (f32[96]{0:T(128)S(1)}, f32[96,256]{1,0:T(8,128)S(1)}) fusion(bf16[2048,256]{1,0:T(8,128)(2,1)} %param.27, bf16[96,2048]{1,0:T(8,128)(2,1)} %param.18, f32[2048]{0:T(1024)S(1)} %bitcast.119, f32[2048]{0:T(1024)S(1)} %bitcast.122, f32[2048]{0:T(1024)} %param.25, f32[96]{0:T(128)S(1)} %add_rsqrt_fusion.2), kind=kOutput, calls=%fused_computation.50 | convolution fusion | flops 101892000 | bytes 1565440 | tf_op jit(solution)/shard_map/dot_general | solution.py:115
  30.3 0.1 multiply_convert_fusion.1
  30.3 8.7 %all_gather.31 = bf16[384,256]{1,0:T(8,128)(2,1)S(1)} all-gather(bf16[96,256]{1,0:T(8,128)(2,1)S(1)} %multiply_convert_fusion.1), channel_id=1, replica_groups=mesh['sp'=4,'tp'=4,'dp'=2] {'tp'}, dimensions={0}, use_global_device_ids=true | all-gather | bytes 245760 | tf_op jit(solution)/shard_map/all_gather | solution.py:126
  39.1 13.8 %all_gather.29 = bf16[512,256]{1,0:T(8,128)(2,1)S(1)} all-gather(bf16[128,256]{1,0:T(8,128)(2,1)S(1)} %copy-done.12), channel_id=1, replica_groups=mesh['sp'=4,'tp'=4,'dp'=2] {'sp'}, dimensions={0}, use_global_device_ids=true | all-gather | bytes 327680 | tf_op jit(solution)/shard_map/all_gather | solution.py:141
  52.9 0.9 convolution_convert_fusion.3
  53.8 0.3 convolution_convert_fusion.1
  54.0 1.0 convolution_convert_fusion
  55.0 0.2 convolution_convert_fusion.2
  55.3 0.6 multiply_reduce_fusion
  55.9 0.1 multiply_convert_fusion
  56.0 8.5 %all_gather.28 = bf16[384,512]{1,0:T(8,128)(2,1)S(1)} all-gather(bf16[96,512]{1,0:T(8,128)(2,1)S(1)} %multiply_convert_fusion), channel_id=1, replica_groups=mesh['sp'=4,'tp'=4,'dp'=2] {'tp'}, dimensions={0}, use_global_device_ids=true | all-gather | bytes 491520 | tf_op jit(solution)/shard_map/all_gather | solution.py:125
  64.5 0.4 fusion.75
  65.0 0.7 slice_negate_fusion.1
  65.7 0.6 fusion.55
  66.3 1.3 fusion.62
  67.6 0.6 copy-done.11
  68.2 0.6 slice_negate_fusion.3
  68.9 0.7 broadcast_multiply_fusion.3
  69.6 0.9 fusion.47
  70.5 8.2 %all-gather = bf16[4,96,64]{1,2,0:T(8,128)(2,1)S(1)} all-gather(bf16[1,96,64]{1,2,0:T(8,128)(2,1)S(1)} %fusion.47), channel_id=1, replica_groups=mesh['sp'=4,'tp'=4,'dp'=2] {'tp'}, dimensions={0}, use_global_device_ids=true | all-gather | bytes 61440 | tf_op jit(solution)/shard_map/all_gather | solution.py:127
  78.7 0.7 copy.48
  79.4 1.6 reshape.254
  81.0 14.6 %all_gather.34 = bf16[1536,64]{0,1:T(8,128)(2,1)S(1)} all-gather(bf16[384,64]{0,1:T(8,128)(2,1)} %reshape.254), channel_id=1, replica_groups=mesh['sp'=4,'tp'=4,'dp'=2] {'sp'}, dimensions={0}, use_global_device_ids=true | all-gather | bytes 245760 | tf_op jit(solution)/shard_map/all_gather | solution.py:194
  95.6 16.9 %all_gather.32 = bf16[1536,256]{1,0:T(8,128)(2,1)S(1)} all-gather(bf16[384,256]{1,0:T(8,128)(2,1)} %convolution_convert_fusion.3), channel_id=1, replica_groups=mesh['sp'=4,'tp'=4,'dp'=2] {'sp'}, dimensions={0}, use_global_device_ids=true | all-gather | bytes 983040 | tf_op jit(solution)/shard_map/all_gather | solution.py:192
  112.5 0.4 fusion.43
  112.9 12.2 %all_gather.30 = bf16[512,64]{0,1:T(8,128)(2,1)S(1)} all-gather(bf16[128,64]{0,1:T(8,128)(2,1)S(1)} %copy-done.13), channel_id=1, replica_groups=mesh['sp'=4,'tp'=4,'dp'=2] {'sp'}, dimensions={0}, use_global_device_ids=true | all-gather | bytes 81920 | tf_op jit(solution)/shard_map/all_gather | solution.py:142
  125.2 0.2 fusion.42
  125.4 0.8 fusion.39
  126.3 1.0 fusion.71
  127.3 0.5 fusion.70
  127.8 0.5 fusion.10
  128.3 15.6 %all_gather.35 = bf16[1536,256]{1,0:T(8,128)(2,1)S(1)} all-gather(bf16[384,256]{1,0:T(8,128)(2,1)S(1)} %convolution_convert_fusion.2), channel_id=1, replica_groups=mesh['sp'=4,'tp'=4,'dp'=2] {'sp'}, dimensions={0}, use_global_device_ids=true | all-gather | bytes 983040 | tf_op jit(solution)/shard_map/all_gather | solution.py:193
  143.8 0.8 fusion.1
  144.7 0.1 copy-done.2
  144.8 0.7 fusion.19
  145.5 0.9 fusion.23
  146.4 0.2 copy.51
  146.6 0.1 all_to_all.14
  146.8 8.1 %all_to_all.19 = bf16[4,96,256]{2,1,0:T(8,128)(2,1)S(1)} all-to-all(bf16[4,96,256]{2,1,0:T(8,128)(2,1)S(1)} %all_to_all.14), channel_id=1, replica_groups=mesh['sp'=4,'tp'=4,'dp'=2] {'tp'}, dimensions={0} | all-to-all | bytes 393216 | tf_op jit(solution)/shard_map/all_to_all | solution.py:200
  154.9 3.8 %fusion.7 = bf16[96,2048]{1,0:T(8,128)(2,1)} fusion(bf16[96,1024]{1,0:T(8,128)(2,1)S(1)} %bitcast.116, bf16[1024,2048]{1,0:T(8,128)(2,1)} %param.35, bf16[96,2048]{1,0:T(8,128)(2,1)S(1)} %copy-done.1, f32[2048]{0:T(1024)S(1)} %bitcast.118), kind=kOutput, calls=%fused_computation.9 | convolution fusion | flops 403439616 | bytes 5185536 | tf_op jit(solution)/shard_map/dot_general | solution.py:201
  (56 shorter events, 0.3 us)
Async XLA Ops:
  0.0 55.3 %copy-start = (bf16[2048,512]{1,0:T(8,128)(2,1)S(1)}, bf16[2048,512]{1,0:T(8,128)(2,1)}, u32[]{:S(2)}) copy-start(bf16[2048,512]{1,0:T(8,128)(2,1)} %param.26) | copy-start | bytes 6291460
  0.0 30.2 %copy-start.19 = (f32[256]{0:T(256)S(1)}, f32[256]{0:T(256)}, u32[]{:S(2)}) copy-start(f32[256]{0:T(256)} %param.30) | copy-start | bytes 3076
  0.0 39.0 %copy-start.12 = (bf16[128,256]{1,0:T(8,128)(2,1)S(1)}, bf16[128,256]{1,0:T(8,128)(2,1)}, u32[]{:S(2)}) copy-start(bf16[128,256]{1,0:T(8,128)(2,1)} %param.20) | copy-start | bytes 196612
  1.3 51.5 %copy-start.3 = (bf16[256,256]{1,0:T(8,128)(2,1)S(1)}, bf16[256,256]{1,0:T(8,128)(2,1)}, u32[]{:S(2)}) copy-start(bf16[256,256]{1,0:T(8,128)(2,1)} %param.32) | copy-start | bytes 393220
  3.8 50.2 %copy-start.4 = (bf16[256,256]{1,0:T(8,128)(2,1)S(1)}, bf16[256,256]{1,0:T(8,128)(2,1)}, u32[]{:S(2)}) copy-start(bf16[256,256]{1,0:T(8,128)(2,1)} %param.33) | copy-start | bytes 393220
  27.1 28.1 %copy-start.14 = (f32[1,2048]{1,0:T(1,128)}, f32[1,2048]{1,0:T(1,128)S(1)}, u32[]{:S(2)}) copy-start(f32[1,2048]{1,0:T(1,128)S(1)} %get-tuple-element.15) | copy-start | bytes 24580
  27.1 27.9 %copy-start.5 = (bf16[256,256]{1,0:T(8,128)(2,1)S(1)}, bf16[256,256]{1,0:T(8,128)(2,1)}, u32[]{:S(2)}) copy-start(bf16[256,256]{1,0:T(8,128)(2,1)} %param.33) | copy-start | bytes 393220
  28.3 26.9 %copy-start.22 = (f32[96]{0:T(128)}, f32[96]{0:T(128)S(1)}, u32[]{:S(2)}) copy-start(f32[96]{0:T(128)S(1)} %add_rsqrt_fusion.2) | copy-start | bytes 1156
  28.3 26.9 %copy-start.1 = (bf16[96,2048]{1,0:T(8,128)(2,1)S(1)}, bf16[96,2048]{1,0:T(8,128)(2,1)}, u32[]{:S(2)}) copy-start(bf16[96,2048]{1,0:T(8,128)(2,1)} %param.18) | copy-start | bytes 1179652
  28.4 26.9 %copy-start.21 = (f32[2048]{0:T(1024)S(1)}, f32[2048]{0:T(1024)}, u32[]{:S(2)}) copy-start(f32[2048]{0:T(1024)} %param.25) | copy-start | bytes 24580
  53.7 2.2 %copy-start.17 = (f32[512]{0:T(512)S(1)}, f32[512]{0:T(512)}, u32[]{:S(2)}) copy-start(f32[512]{0:T(512)} %param.29) | copy-start | bytes 6148
  54.0 10.5 %copy-start.6 = (bf16[512,384]{1,0:T(8,128)(2,1)S(1)}, bf16[512,384]{1,0:T(8,128)(2,1)}, u32[]{:S(2)}) copy-start(bf16[512,384]{1,0:T(8,128)(2,1)} %param.31) | copy-start | bytes 1179652
  67.6 0.6 copy-start.11
  70.5 54.6 %copy-start.15 = (f32[384]{0:T(512)S(1)}, f32[384]{0:T(512)}, u32[]{:S(2)}) copy-start(f32[384]{0:T(512)} %get-tuple-element.33) | copy-start | bytes 4612
  70.5 54.6 %copy-start.16 = (f32[384]{0:T(512)S(1)}, f32[384]{0:T(512)}, u32[]{:S(2)}) copy-start(f32[384]{0:T(512)} %get-tuple-element.34) | copy-start | bytes 4612
  81.0 31.9 %copy-start.13 = (bf16[128,64]{0,1:T(8,128)(2,1)S(1)}, bf16[128,64]{0,1:T(8,128)(2,1)}, u32[]{:S(2)}) copy-start(bf16[128,64]{0,1:T(8,128)(2,1)} %param.21) | copy-start | bytes 49156
  81.0 44.1 %copy-start.18 = (f32[16]{0:T(128)S(1)}, f32[16]{0:T(128)}, u32[]{:S(2)}) copy-start(f32[16]{0:T(128)} %multiply_power_fusion) | copy-start | bytes 196
  81.0 44.4 %copy-start.7 = (f32[384,2,16]{0,2,1:T(8,128)S(1)}, f32[384,2,16]{0,2,1:T(8,128)}, u32[]{:S(2)}) copy-start(f32[384,2,16]{0,2,1:T(8,128)} %get-tuple-element.7) | copy-start | bytes 147460
  81.0 44.4 %copy-start.8 = (f32[384,2,16]{0,2,1:T(8,128)S(1)}, f32[384,2,16]{0,2,1:T(8,128)}, u32[]{:S(2)}) copy-start(f32[384,2,16]{0,2,1:T(8,128)} %get-tuple-element.8) | copy-start | bytes 147460
  81.0 44.4 %copy-start.9 = (f32[384,2,16]{0,2,1:T(8,128)S(1)}, f32[384,2,16]{0,2,1:T(8,128)}, u32[]{:S(2)}) copy-start(f32[384,2,16]{0,2,1:T(8,128)} %get-tuple-element.9) | copy-start | bytes 147460
  81.0 44.4 %copy-start.10 = (f32[384,2,16]{0,2,1:T(8,128)S(1)}, f32[384,2,16]{0,2,1:T(8,128)}, u32[]{:S(2)}) copy-start(f32[384,2,16]{0,2,1:T(8,128)} %get-tuple-element.10) | copy-start | bytes 147460
  126.3 1.0 copy-start.20
  143.8 1.0 copy-start.2
where the time goes:
time: 159 us
  blocking collectives  129 us (81%)
  matrix products  18.4 us (12%)
  other arithmetic  7.9 us (5%)
  local copies, waits for them, and re-layouts  3.43 us (2%)
    all_gather x1, blocking collectives, on_device(): lax.all_gather(own_nope, 'sp', axis=0, tiled=True)  16.9 us
    all_gather x1, blocking collectives, on_device(): lax.all_gather(own_values, 'sp', axis=0, tiled=True)  15.6 us
    all_gather x1, blocking collectives, on_device(): lax.all_gather(rope_group, 'sp', axis=0, tiled=True)  14.6 us
    all_gather x1, blocking collectives, on_device(): lax.all_gather(context_latent, 'sp', axis=0, tiled=True)  13.8 us
    psum x1, blocking collectives, on_device(): summed = lax.psum(partials, 'sp')  13.8 us
    all_gather x1, blocking collectives, on_device(): lax.all_gather(context_rope, 'sp', axis=0, tiled=True)  12.2 us
    all_gather x1, blocking collectives, on_device(): lax.all_gather(latent_low, 'tp', axis=0, tiled=True)  8.7 us
    all_gather x1, blocking collectives, on_device(): lax.all_gather(query_low, 'tp', axis=0, tiled=True)  8.53 us

commit v1 on v0

--- a/solution.py
+++ b/solution.py
@@ -99,7 +99,9 @@
             for weight_in in (shift_weight, scale_weight, gate_weight)
         ]
     )
-    summed = lax.psum(partials, "sp")
+    summed = partials
+    for hop in (1, 2):
+        summed = summed + lax.ppermute(summed, "sp", [(dev, dev ^ hop) for dev in range(4)])
     modulation = lax.all_gather(summed, "tp", axis=1, tiled=True)
     shift_vec = modulation[0]
     scale_vec = modulation[1]

time: 159 us -> 148 us (0.931)
  blocking collectives: 129 us -> 118 us
  starting transfers between devices: 0 us -> 3.84 us
  other arithmetic: 7.9 us -> 5.42 us
    psum x1 -> x0, blocking collectives: 13.8 us -> none  [on_device(): summed = lax.psum(partials, 'sp')]
    ppermute x0 -> x2, starting transfers between devices: none -> 3.84 us  [on_device(): lax.ppermute(summed, 'sp', [(dev, dev ^ hop) for dev in range(4)])]
  transfers between devices with their start and end apart: 0 -> 2, of which waited for: 0 -> 0; matrix products, arithmetic and copies ran while one was open for 0% -> 2% of each run, Pallas kernels for 0% -> 0%
where the time goes in v1:
time: 148 us
  blocking collectives  118 us (80%)
  matrix products  17.2 us (12%)
  other arithmetic  5.42 us (4%)
  starting transfers between devices  3.84 us (3%)
  local copies, waits for them, and re-layouts  2.8 us (2%)
    all_gather x1, blocking collectives, on_device(): lax.all_gather(own_nope, 'sp', axis=0, tiled=True)  18.1 us
    all_gather x1, blocking collectives, on_device(): lax.all_gather(own_values, 'sp', axis=0, tiled=True)  15.7 us
    all_gather x1, blocking collectives, on_device(): lax.all_gather(rope_group, 'sp', axis=0, tiled=True)  14.6 us
    all_gather x1, blocking collectives, on_device(): lax.all_gather(context_latent, 'sp', axis=0, tiled=True)  14.3 us
    all_gather x1, blocking collectives, on_device(): lax.all_gather(context_rope, 'sp', axis=0, tiled=True)  12.6 us
    all_gather x1, blocking collectives, on_device(): lax.all_gather(latent_low, 'tp', axis=0, tiled=True)  9.45 us
    all_gather x1, blocking collectives, on_device(): lax.all_gather(rope_keys, 'tp', axis=0, tiled=True)  8.84 us
    all_gather x1, blocking collectives, on_device(): modulation = lax.all_gather(summed, 'tp', axis=1, tiled=True)  8.2 us
  transfers between devices with their start and end apart: 2, of which 0 were waited for; matrix products, arithmetic and copies ran while one was open for 2% of the time, Pallas kernels for 0%

profile of v1, /device:TPU:0, one launch (start us, length us, event | category | flops | bytes accessed | tf_op | source)
XLA Modules:
  0.0 147.6 jit_solution(17192571535624305825)
XLA Ops:
  0.0 0.8 fusion.53
  0.9 1.3 fusion.72
  2.1 1.2 fusion.73
  3.4 1.2 fusion.74
  4.6 3.1 %collective-permute-start = (f32[3,512]{1,0:T(4,128)S(1)}, f32[3,512]{1,0:T(4,128)S(1)}, u32[]{:S(2)}, u32[]{:S(2)}) collective-permute-start(f32[3,512]{1,0:T(4,128)S(1)} %pad_maximum_fusion.2), channel_id=1, source_target_pairs={{0,8},{8,0},{16,24},{24,16},{1,9},{9,1},{17,25},{25,17},{2,10},{10... | collective-permute-start | bytes 18440 | tf_op jit(solution)/shard_map/ppermute | solution.py:104
  7.7 1.2 fusion.24
  9.0 14.3 %all_gather.29 = bf16[512,256]{1,0:T(8,128)(2,1)S(1)} all-gather(bf16[128,256]{1,0:T(8,128)(2,1)} %param.20), channel_id=1, replica_groups=mesh['sp'=4,'tp'=4,'dp'=2] {'sp'}, dimensions={0}, use_global_device_ids=true | all-gather | bytes 327680 | tf_op jit(solution)/shard_map/all_gather | solution.py:143
  23.3 0.3 convolution_convert_fusion.1
  23.6 1.0 convolution_convert_fusion
  24.6 0.1 broadcast_multiply_fusion.1
  24.6 0.1 broadcast_multiply_fusion.3
  24.7 0.9 fusion.41
  25.6 0.7 collective-permute-start.1
  26.3 12.6 %all_gather.30 = bf16[512,64]{0,1:T(8,128)(2,1)} all-gather(bf16[128,64]{0,1:T(8,128)(2,1)S(1)} %copy-done.13), channel_id=1, replica_groups=mesh['sp'=4,'tp'=4,'dp'=2] {'sp'}, dimensions={0}, use_global_device_ids=true | all-gather | bytes 81920 | tf_op jit(solution)/shard_map/all_gather | solution.py:144
  38.9 8.2 %all_gather.27 = f32[3,2048]{1,0:T(4,128)S(1)} all-gather(f32[3,512]{1,0:T(4,128)S(1)} %fusion.101), channel_id=1, replica_groups=mesh['sp'=4,'tp'=4,'dp'=2] {'tp'}, dimensions={1}, use_global_device_ids=true | all-gather | bytes 30720 | tf_op jit(solution)/shard_map/all_gather | solution.py:105
  47.2 1.7 %multiply_reduce_fusion.1 = (f32[96]{0:T(128)S(1)}, f32[96,256]{1,0:T(8,128)S(1)}) fusion(bf16[2048,256]{1,0:T(8,128)(2,1)} %param.27, bf16[96,2048]{1,0:T(8,128)(2,1)S(1)} %copy-done.1, f32[2048]{0:T(1024)S(1)} %bitcast.119, f32[2048]{0:T(1024)S(1)} %bitcast.122, f32[2048]{0:T(1024)S(1)} %copy-done.18, f32[96]{0:T(128)S(1)} %add_rsqrt_fusion.2), kind=kOutput, calls=%fused_computation.49 | convolution fusion | flops 101892000 | bytes 1565440 | tf_op jit(solution)/shard_map/dot_general | solution.py:117
  48.9 0.0 copy-start.14
  48.9 0.1 multiply_convert_fusion.1
  49.0 9.4 %all_gather.31 = bf16[384,256]{1,0:T(8,128)(2,1)S(1)} all-gather(bf16[96,256]{1,0:T(8,128)(2,1)S(1)} %multiply_convert_fusion.1), channel_id=1, replica_groups=mesh['sp'=4,'tp'=4,'dp'=2] {'tp'}, dimensions={0}, use_global_device_ids=true | all-gather | bytes 245760 | tf_op jit(solution)/shard_map/all_gather | solution.py:128
  58.4 0.9 convolution_convert_fusion.3
  59.3 0.2 convolution_convert_fusion.2
  59.6 0.0 copy-start.17
  59.6 0.6 multiply_reduce_fusion
  60.2 0.1 multiply_convert_fusion
  60.3 8.1 %all_gather.28 = bf16[384,512]{1,0:T(8,128)(2,1)S(1)} all-gather(bf16[96,512]{1,0:T(8,128)(2,1)S(1)} %multiply_convert_fusion), channel_id=1, replica_groups=mesh['sp'=4,'tp'=4,'dp'=2] {'tp'}, dimensions={0}, use_global_device_ids=true | all-gather | bytes 491520 | tf_op jit(solution)/shard_map/all_gather | solution.py:127
  68.4 0.4 fusion.75
  68.8 0.7 slice_negate_fusion.1
  69.5 0.4 fusion.62
  69.9 0.1 fusion.46
  70.0 8.8 %all-gather = bf16[4,96,64]{1,2,0:T(8,128)(2,1)S(1)} all-gather(bf16[1,96,64]{1,2,0:T(8,128)(2,1)S(1)} %fusion.46), channel_id=1, replica_groups=mesh['sp'=4,'tp'=4,'dp'=2] {'tp'}, dimensions={0}, use_global_device_ids=true | all-gather | bytes 61440 | tf_op jit(solution)/shard_map/all_gather | solution.py:129
  78.8 0.7 copy.48
  79.5 1.6 %reshape.254 = bf16[384,64]{0,1:T(8,128)(2,1)} reshape(bf16[4,96,64]{1,0,2:T(4,128)(2,1)} %copy.48) | data formatting | bytes 98304
  81.1 14.6 %all_gather.34 = bf16[1536,64]{0,1:T(8,128)(2,1)S(1)} all-gather(bf16[384,64]{0,1:T(8,128)(2,1)} %reshape.254), channel_id=1, replica_groups=mesh['sp'=4,'tp'=4,'dp'=2] {'sp'}, dimensions={0}, use_global_device_ids=true | all-gather | bytes 245760 | tf_op jit(solution)/shard_map/all_gather | solution.py:196
  95.7 18.1 %all_gather.32 = bf16[1536,256]{1,0:T(8,128)(2,1)S(1)} all-gather(bf16[384,256]{1,0:T(8,128)(2,1)} %convolution_convert_fusion.3), channel_id=1, replica_groups=mesh['sp'=4,'tp'=4,'dp'=2] {'sp'}, dimensions={0}, use_global_device_ids=true | all-gather | bytes 983040 | tf_op jit(solution)/shard_map/all_gather | solution.py:194
  113.8 0.4 fusion.42
  114.4 0.8 fusion.38
  115.2 1.0 fusion.71
  116.2 0.5 fusion.70
  116.7 0.5 fusion.8
  117.2 15.7 %all_gather.35 = bf16[1536,256]{1,0:T(8,128)(2,1)S(1)} all-gather(bf16[384,256]{1,0:T(8,128)(2,1)S(1)} %convolution_convert_fusion.2), channel_id=1, replica_groups=mesh['sp'=4,'tp'=4,'dp'=2] {'sp'}, dimensions={0}, use_global_device_ids=true | all-gather | bytes 983040 | tf_op jit(solution)/shard_map/all_gather | solution.py:195
  132.9 0.8 fusion.1
  133.7 0.1 copy-done.2
  133.8 0.7 fusion.17
  134.5 0.9 fusion.21
  135.4 0.2 copy.51
  135.6 0.1 all_to_all.14
  135.8 8.1 %all_to_all.19 = bf16[4,96,256]{2,1,0:T(8,128)(2,1)S(1)} all-to-all(bf16[4,96,256]{2,1,0:T(8,128)(2,1)S(1)} %all_to_all.14), channel_id=1, replica_groups=mesh['sp'=4,'tp'=4,'dp'=2] {'tp'}, dimensions={0} | all-to-all | bytes 393216 | tf_op jit(solution)/shard_map/all_to_all | solution.py:202
  143.9 3.8 %fusion.29 = bf16[96,2048]{1,0:T(8,128)(2,1)} fusion(bf16[96,2048]{1,0:T(8,128)(2,1)S(1)} %copy-done.1, f32[2048]{0:T(1024)S(1)} %bitcast.118, bf16[96,1024]{1,0:T(8,128)(2,1)S(1)} %bitcast.116, bf16[1024,2048]{1,0:T(8,128)(2,1)} %param.35), kind=kOutput, calls=%fused_computation.32 | convolution fusion | flops 403439616 | bytes 5185536 | tf_op jit(solution)/shard_map/dot_general | solution.py:203
  (57 shorter events, 0.3 us)
Async XLA Ops:
  0.0 59.6 %copy-start = (bf16[2048,512]{1,0:T(8,128)(2,1)S(1)}, bf16[2048,512]{1,0:T(8,128)(2,1)}, u32[]{:S(2)}) copy-start(bf16[2048,512]{1,0:T(8,128)(2,1)} %param.26) | copy-start | bytes 6291460
  0.0 47.2 %copy-start.1 = (bf16[96,2048]{1,0:T(8,128)(2,1)S(1)}, bf16[96,2048]{1,0:T(8,128)(2,1)}, u32[]{:S(2)}) copy-start(bf16[96,2048]{1,0:T(8,128)(2,1)} %param.18) | copy-start | bytes 1179652
  0.0 23.3 %copy-start.3 = (bf16[256,256]{1,0:T(8,128)(2,1)S(1)}, bf16[256,256]{1,0:T(8,128)(2,1)}, u32[]{:S(2)}) copy-start(bf16[256,256]{1,0:T(8,128)(2,1)} %param.32) | copy-start | bytes 393220
  0.0 23.6 %copy-start.4 = (bf16[256,256]{1,0:T(8,128)(2,1)S(1)}, bf16[256,256]{1,0:T(8,128)(2,1)}, u32[]{:S(2)}) copy-start(bf16[256,256]{1,0:T(8,128)(2,1)} %param.33) | copy-start | bytes 393220
  0.0 26.3 %copy-start.13 = (bf16[128,64]{0,1:T(8,128)(2,1)S(1)}, bf16[128,64]{0,1:T(8,128)(2,1)}, u32[]{:S(2)}) copy-start(bf16[128,64]{0,1:T(8,128)(2,1)} %param.21) | copy-start | bytes 49156
  0.0 47.2 %copy-start.18 = (f32[2048]{0:T(1024)S(1)}, f32[2048]{0:T(1024)}, u32[]{:S(2)}) copy-start(f32[2048]{0:T(1024)} %param.25) | copy-start | bytes 24580
  4.6 44.3 %copy-start.15 = (f32[256]{0:T(256)S(1)}, f32[256]{0:T(256)}, u32[]{:S(2)}) copy-start(f32[256]{0:T(256)} %param.30) | copy-start | bytes 3076
  4.6 21.0 %collective-permute-start = (f32[3,512]{1,0:T(4,128)S(1)}, f32[3,512]{1,0:T(4,128)S(1)}, u32[]{:S(2)}, u32[]{:S(2)}) collective-permute-start(f32[3,512]{1,0:T(4,128)S(1)} %pad_maximum_fusion.2), channel_id=1, source_target_pairs={{0,8},{8,0},{16,24},{24,16},{1,9},{9,1},{17,25},{25,17},{2,10},{10... | collective-permute-start | bytes 18440 | tf_op jit(solution)/shard_map/ppermute | solution.py:104
  8.9 50.6 %copy-start.19 = (f32[96]{0:T(128)}, f32[96]{0:T(128)S(1)}, u32[]{:S(2)}) copy-start(f32[96]{0:T(128)S(1)} %add_rsqrt_fusion.2) | copy-start | bytes 1156
  25.6 13.3 %collective-permute-start.1 = (f32[3,512]{1,0:T(4,128)S(1)}, f32[3,512]{1,0:T(4,128)S(1)}, u32[]{:S(2)}, u32[]{:S(2)}) collective-permute-start(f32[3,512]{1,0:T(4,128)S(1)} %fusion.61), channel_id=1, source_target_pairs={{0,16},{8,24},{16,0},{24,8},{1,17},{9,25},{17,1},{25,9},{2,18},{10... | collective-permute-start | bytes 18440 | tf_op jit(solution)/shard_map/ppermute | solution.py:104
  48.9 11.3 %copy-start.14 = (f32[512]{0:T(512)S(1)}, f32[512]{0:T(512)}, u32[]{:S(2)}) copy-start(f32[512]{0:T(512)} %param.29) | copy-start | bytes 6148
  58.4 10.0 %copy-start.5 = (bf16[512,384]{1,0:T(8,128)(2,1)S(1)}, bf16[512,384]{1,0:T(8,128)(2,1)}, u32[]{:S(2)}) copy-start(bf16[512,384]{1,0:T(8,128)(2,1)} %param.31) | copy-start | bytes 1179652
  59.6 9.9 %copy-start.17 = (bf16[2048,64]{0,1:T(8,128)(2,1)S(1)}, bf16[2048,64]{0,1:T(8,128)(2,1)}, u32[]{:S(2)}) copy-start(bf16[2048,64]{0,1:T(8,128)(2,1)} %param.28) | copy-start | bytes 786436
  60.2 9.3 %copy-start.20 = (f32[96]{0:T(128)S(1)}, f32[96]{0:T(128)}, u32[]{:S(2)}) copy-start(f32[96]{0:T(128)} %copy-done.19) | copy-start | bytes 1156
  81.1 33.2 %copy-start.6 = (f32[384,64]{0,1:T(8,128)S(1)}, f32[384,64]{0,1:T(8,128)}, u32[]{:S(2)}) copy-start(f32[384,64]{0,1:T(8,128)} %get-tuple-element.11) | copy-start | bytes 294916
  81.1 33.2 %copy-start.7 = (f32[384,64]{0,1:T(8,128)S(1)}, f32[384,64]{0,1:T(8,128)}, u32[]{:S(2)}) copy-start(f32[384,64]{0,1:T(8,128)} %get-tuple-element.12) | copy-start | bytes 294916
  81.1 33.2 %copy-start.9 = (f32[384,2,16]{0,2,1:T(8,128)S(1)}, f32[384,2,16]{0,2,1:T(8,128)}, u32[]{:S(2)}) copy-start(f32[384,2,16]{0,2,1:T(8,128)} %get-tuple-element.7) | copy-start | bytes 147460
  81.1 33.2 %copy-start.10 = (f32[384,2,16]{0,2,1:T(8,128)S(1)}, f32[384,2,16]{0,2,1:T(8,128)}, u32[]{:S(2)}) copy-start(f32[384,2,16]{0,2,1:T(8,128)} %get-tuple-element.8) | copy-start | bytes 147460
  81.1 33.2 %copy-start.11 = (f32[384,2,16]{0,2,1:T(8,128)S(1)}, f32[384,2,16]{0,2,1:T(8,128)}, u32[]{:S(2)}) copy-start(f32[384,2,16]{0,2,1:T(8,128)} %get-tuple-element.9) | copy-start | bytes 147460
  81.1 33.2 %copy-start.12 = (f32[384,2,16]{0,2,1:T(8,128)S(1)}, f32[384,2,16]{0,2,1:T(8,128)}, u32[]{:S(2)}) copy-start(f32[384,2,16]{0,2,1:T(8,128)} %get-tuple-element.10) | copy-start | bytes 147460
  115.2 1.0 copy-start.8
  115.2 1.0 copy-start.16
  132.9 1.0 copy-start.2
